TPU v7x, 32 devices: a whole 2x2x4 slice. The times are simulated.
32 devices in a mesh: grp: 2 (over y), sp: 16 (over z, x, core), tp: 1.
Axes of the slice: x: 2, y: 2, z: 4, core: 2. Of those that a mesh axis runs over, the one named last changes fastest.
Arguments:
- resid: bfloat16 [8192, 2048], P(('grp', 'sp', 'tp')), parts along dimension 0, may hold values from -6 to 6
- gate_b: bfloat16 [8192, 2048], P(('grp', 'sp'), 'tp'), parts along dimension 0, may hold values from -6 to 6
- gate_c: bfloat16 [8192, 2048], P(('grp', 'sp'), 'tp'), parts along dimension 0, may hold values from -6 to 6
- value: bfloat16 [8192, 2048], P(('grp', 'sp'), 'tp'), parts along dimension 0, may hold values from -6 to 6
- taps: bfloat16 [3, 2048], P(None, 'tp'), may hold values from -3.5 to 3.5
- doc_ids: int32 [8192], P(('grp', 'sp')), parts along dimension 0, may hold values from 0 to 3, never falling along the last dimension, each value on 1 to 2048 neighbouring positions
- out_weight: bfloat16 [2048, 2048], P('tp'), may hold values from -0.125 to 0.125
- norm_gains: float32 [3, 2048], replicated, may hold values from 0.1 to 1.9
- routes: int32 [8192, 2], P(('grp', 'sp')), parts along dimension 0, may hold values from 0 to 15, all different within a row; in each aligned block of 256 rows (0 to 255, 256 to 511, ...) at most 48 rows name the same one
- route_weights: float32 [8192, 2], P(('grp', 'sp')), parts along dimension 0, may hold values from 0.2 to 1
- w_gate: bfloat16 [16, 2048, 4096], P('sp', None, 'tp'), may hold values from -0.125 to 0.125
- w_up: bfloat16 [16, 2048, 4096], P('sp', None, 'tp'), may hold values from -0.125 to 0.125
- w_down: bfloat16 [16, 4096, 2048], P('sp', 'tp'), may hold values from -0.09375 to 0.09375
Outputs:
- layer_out: bfloat16 [8192, 2048], P(('grp', 'sp', 'tp')), parts along dimension 0
There are 2 independent parts, one for each index of `grp`. A program takes and returns all parts, laid end to end along the dimension named above; an argument that names none is the same for every part. Nothing has to cross between parts.
Inputs may be any that keep to these rules, and one draw needn't show every extreme that they name: `doc_ids`: never falling along the sequence; each document spans 1 to 2048 positions. `routes`: each row names 2 different experts. In each aligned block of 256 rows no expert is named more than 48 times, and in every draw some block names some expert exactly 48 times.
All inputs are finite; a program needn't handle non-finite values.
Results may differ from a plain program's by a relative error of at most 0.02.
Values may be sent and summed in bfloat16 or wider, within the bound.
A program may use at most 128 MiB of HBM per device.

v0:
```python
import jax
import jax.numpy as jnp
from jax import lax
from jax.sharding import PartitionSpec as P

TAPS = 3
TOP = 2


norm_eps = 1e-06


def passed_along(block, axis, distance):
    devices = range(lax.axis_size(axis))
    route = [(i - distance, i) for i in devices if i - distance in devices]
    return lax.ppermute(block, axis, route)


def rms_scale(values, gain_row):
    mean_sq = jnp.mean(values * values, axis=-1, keepdims=True)
    return values * lax.rsqrt(mean_sq + norm_eps) * gain_row


def slot_table(block_routes, experts, capacity):
    block_count = block_routes.shape[0]
    block_len = block_routes.shape[1]
    flat_routes = block_routes.reshape(block_count, block_len * TOP)
    onehot = (
        flat_routes[:, :, None] == jnp.arange(experts, dtype=jnp.int32)[None, None, :]
    ).astype(jnp.int32)
    before = jnp.cumsum(onehot, axis=1) - onehot
    slot_rank = jnp.sum(before * onehot, axis=2)
    slot_hit = onehot[:, :, :, None] * (
        slot_rank[:, :, None, None] == jnp.arange(capacity, dtype=jnp.int32)[None, None, None, :]
    ).astype(jnp.int32)
    owner_row = jnp.arange(block_len * TOP, dtype=jnp.int32) // TOP
    slot_tok = jnp.sum(slot_hit * owner_row[None, :, None, None], axis=1)
    filled = jnp.sum(slot_hit, axis=1)
    return (slot_rank.reshape(block_count, block_len, TOP), slot_tok, filled)


def pick_rows(normed_rows, slot_tok, filled):
    picked_rows = normed_rows[slot_tok]
    return jnp.where(filled[:, :, None] > 0, picked_rows, jnp.zeros_like(picked_rows))


def expert_hidden(picked_rows, w_gate, w_up):
    gate_proj = jnp.dot(picked_rows, w_gate[0], preferred_element_type=jnp.float32)
    up_proj = jnp.dot(picked_rows, w_up[0], preferred_element_type=jnp.float32)
    return (jax.nn.silu(gate_proj) * up_proj).astype(jnp.bfloat16)


def per_device(
    resid,
    gate_b,
    gate_c,
    value,
    taps,
    doc_ids,
    out_weight,
    norm_gains,
    routes,
    route_weights,
    w_gate,
    w_up,
    w_down,
):
    tok_dev = gate_b.shape[0]
    rows_blk = resid.shape[0]
    model_width = resid.shape[1]
    experts = lax.axis_size("sp")
    capacity = max(2, 3 * TOP * rows_blk // (2 * experts))
    tap_reach = TAPS - 1
    product = gate_c.astype(jnp.float32) * value.astype(jnp.float32)
    id_values = doc_ids.astype(jnp.float32)
    prev_rows, prev_ids = passed_along(
        (product[tok_dev - tap_reach :], id_values[tok_dev - tap_reach :]), "sp", 1
    )
    ext_rows = jnp.concatenate([prev_rows, product], axis=0)
    ext_ids = jnp.concatenate([prev_ids, id_values], axis=0)
    tap_weights = taps.astype(jnp.float32)
    convolved = tap_weights[0] * product
    for distance in range(1, TAPS):
        earlier = ext_rows[tap_reach - distance : tap_reach - distance + tok_dev]
        same_doc = ext_ids[tap_reach - distance : tap_reach - distance + tok_dev] == id_values
        convolved = convolved + jnp.where(same_doc[:, None], tap_weights[distance] * earlier, 0.0)
    mixed_rows = (gate_b.astype(jnp.float32) * convolved).astype(jnp.bfloat16)
    block_rows = mixed_rows
    projected = lax.psum_scatter(
        jnp.dot(block_rows, out_weight, preferred_element_type=jnp.float32).astype(jnp.bfloat16),
        "tp",
        scatter_dimension=0,
        tiled=True,
    ).astype(jnp.float32)
    stream = resid.astype(jnp.float32) + rms_scale(projected, norm_gains[0])
    normed = rms_scale(stream, norm_gains[1]).astype(jnp.bfloat16)
    lane_index = lax.axis_index("tp")
    offset = lane_index * rows_blk
    my_routes = lax.dynamic_slice_in_dim(routes, offset, rows_blk, 0)
    my_weights = lax.dynamic_slice_in_dim(route_weights, offset, rows_blk, 0)
    own_rank, own_tok, own_filled = slot_table(my_routes[None], experts, capacity)
    slot_rank = own_rank[0]
    outgoing = pick_rows(normed, own_tok[0], own_filled[0])
    arrived = lax.all_to_all(outgoing, "sp", split_axis=0, concat_axis=0, tiled=True)
    hidden = expert_hidden(
        lax.all_gather(arrived[None], "tp", axis=0, tiled=True).reshape(-1, model_width),
        w_gate,
        w_up,
    )
    block_rows = hidden
    summed = lax.psum_scatter(
        jnp.dot(block_rows, w_down[0], preferred_element_type=jnp.float32).astype(jnp.bfloat16),
        "tp",
        scatter_dimension=0,
        tiled=True,
    )
    results = summed.reshape(experts, capacity, model_width)
    returned = lax.all_to_all(results, "sp", split_axis=0, concat_axis=0, tiled=True)
    picked = returned[my_routes, slot_rank]
    shares = my_weights / jnp.sum(my_weights, axis=1, keepdims=True)
    combined = jnp.sum(shares[:, :, None] * picked.astype(jnp.float32), axis=1)
    return (stream + rms_scale(combined, norm_gains[2])).astype(jnp.bfloat16)


def solution(mesh):
    return jax.shard_map(
        per_device,
        mesh=mesh,
        in_specs=(
            P(("grp", "sp", "tp"), None),
            P(("grp", "sp"), "tp"),
            P(("grp", "sp"), "tp"),
            P(("grp", "sp"), "tp"),
            P(None, "tp"),
            P(("grp", "sp")),
            P("tp", None),
            P(),
            P(("grp", "sp"), None),
            P(("grp", "sp"), None),
            P("sp", None, "tp"),
            P("sp", None, "tp"),
            P("sp", "tp", None),
        ),
        out_specs=P(("grp", "sp", "tp"), None),
        check_vma=False,
    )
```

profile of v0, /device:TPU:11, one launch (start us, length us, event | category | flops | bytes accessed | tf_op | source)
XLA Modules:
  0.0 265.3 jit_solution(12587690889693497333)
XLA Ops:
  0.0 0.7 convert_element_type.72
  0.8 3.9 %collective-permute-start = (f32[2]{0:T(128)S(1)}, f32[2]{0:T(128)S(1)}, u32[]{:S(2)}, u32[]{:S(2)}) collective-permute-start(f32[2]{0:T(128)S(1)} %slice.43), channel_id=1, source_target_pairs={{0,1},{1,2},{2,3},{3,4},{4,5},{5,6},{6,7},{7,8},{8,9},{9,10},{10,1... | collective-permute-start | bytes 32 | tf_op jit(solution)/shard_map/ppermute | solution.py:16
  4.6 1.9 convert_multiply_fusion.2
  6.6 1.9 collective-permute-start.1
  8.8 1.2 reduce-window.6
  10.6 0.6 multiply_reduce_fusion.1
  11.6 6.8 %fusion.23 = (f32[256]{0:T(256)S(1)}, bf16[256,2048]{1,0:T(8,128)(2,1)S(1)}) fusion(bf16[2048,2048]{1,0:T(8,128)(2,1)} %param.19, f32[2,2048]{1,0:T(2,128)S(1)} %collective-permute-done.1, f32[256,2048]{1,0:T(8,128)S(1)} %convert_multiply_fusion.2, bf16[256,2048]{1,0:T(8,128)(2,1)} %param.14, f32[2048]{0:T(1024)S(1)} %bitcast.68, f32[2048]{0:T(1024)S(1)} %bitcast.67, ...), kind=kOutput, calls=%fused_computation.27 | convolution fusion | flops 2155872000 | bytes 12625408 | tf_op jit(solution)/shard_map/dot_general | solution.py:90
  18.4 0.6 multiply_reduce_fusion.3
  19.0 0.3 copy-done.2
  19.3 0.6 multiply_convert_fusion.1
  20.0 4.3 %gather_fusion = bf16[768,2048]{1,0:T(8,128)(2,1)} fusion(bf16[256,2048]{1,0:T(8,128)(2,1)S(1)} %multiply_convert_fusion.1, s32[1024]{0:T(1024)S(1)} %pad_clamp_fusion), kind=kCustom, calls=%fused_computation | custom fusion | bytes 6294528 | tf_op jit(solution)/shard_map/gather | solution.py:43
  24.2 2.2 broadcast_select_fusion
  26.4 74.9 %all_to_all.10 = bf16[16,48,2048]{2,1,0:T(8,128)(2,1)S(1)} all-to-all(bf16[16,48,2048]{2,1,0:T(8,128)(2,1)S(1)} %broadcast_select_fusion), channel_id=1, replica_groups=mesh['grp'=2,'sp'=16,'tp'=1] {'sp'}, dimensions={0} | all-to-all | bytes 6291456 | tf_op jit(solution)/shard_map/all_to_all | solution.py:104
  101.3 19.3 %fusion.4 = f32[768,4096]{1,0:T(8,128)} fusion(bf16[768,2048]{1,0:T(8,128)(2,1)S(1)} %bitcast.55, bf16[1,2048,4096]{2,1,0:T(8,128)(2,1)} %param.23), kind=kOutput, calls=%fused_computation.6 | convolution fusion | flops 12884901888 | bytes 32505856 | tf_op jit(solution)/shard_map/dot_general | solution.py:48
  120.7 40.4 %fusion.11 = bf16[768,2048]{1,0:T(8,128)(2,1)} fusion(bf16[1,4096,2048]{2,1,0:T(8,128)(2,1)} %param.25, f32[768,4096]{1,0:T(8,128)} %fusion.4, bf16[768,2048]{1,0:T(8,128)(2,1)S(1)} %bitcast.56, bf16[1,2048,4096]{2,1,0:T(8,128)(2,1)} %param.24), kind=kOutput, calls=%fused_computation.11 | convolution fusion | flops 25790251008 | bytes 52428800 | tf_op jit(solution)/shard_map/dot_general | solution.py:112
  161.1 5.2 %all-to-all-start.1 = ((bf16[16,48,2048]{2,1,0:T(8,128)(2,1)}), bf16[16,48,2048]{2,1,0:T(8,128)(2,1)S(1)}, u32[]{:S(2)}, u32[]{:S(2)}) async-start(bf16[16,48,2048]{2,1,0:T(8,128)(2,1)} %bitcast.54), calls=%async_computation.1 | async-start | bytes 6291456 | tf_op jit(solution)/shard_map/all_to_all | solution.py:118
  167.1 69.2 %all-to-all-done.1 = bf16[16,48,2048]{2,1,0:T(8,128)(2,1)S(1)} async-done(((bf16[16,48,2048]{2,1,0:T(8,128)(2,1)}), bf16[16,48,2048]{2,1,0:T(8,128)(2,1)S(1)}, u32[]{:S(2)}, u32[]{:S(2)}) %all-to-all-start.1) | async-done | bytes 3145760 | tf_op jit(solution)/shard_map/all_to_all | solution.py:118
  236.2 11.5 %gather_fusion.1 = bf16[512,2048]{1,0:T(8,128)(2,1)} fusion(bf16[16,48,2048]{2,1,0:T(8,128)(2,1)S(1)} %all-to-all-done.1, s32[512]{0:T(512)S(1)} %reshape.289), kind=kCustom, calls=%fused_computation.1 | custom fusion | bytes 4198400 | tf_op jit(solution)/shard_map/gather | solution.py:119
  247.7 5.4 %reshape.296 = f32[256,2,2048]{2,1,0:T(2,128)} reshape(bf16[512,2048]{1,0:T(8,128)(2,1)} %gather_fusion.1) | data formatting | bytes 6291456 | tf_op jit(solution)/shard_map/convert_element_type | solution.py:121
  253.2 8.9 %multiply_reduce_fusion = f32[256,2048]{1,0:T(8,128)S(1)} fusion(f32[256,2,2048]{2,1,0:T(2,128)} %reshape.296, f32[256,2]{1,0:T(8,128)S(1)} %copy.35), kind=kLoop, calls=%fused_computation.10 | loop fusion | flops 1572864 | bytes 6293504 | tf_op jit(solution)/shard_map/reduce_sum | solution.py:121
  262.1 0.2 multiply_reduce_fusion.2
  262.3 1.0 copy-done.1
  263.3 0.3 copy-done.3
  263.6 1.7 add_convert_fusion
  (52 shorter events, 2.0 us)
Async XLA Ops:
  0.8 7.7 %copy-start.6 = (s32[256,2]{0,1:T(2,128)S(1)}, s32[256,2]{0,1:T(2,128)}, u32[]{:S(2)}) copy-start(s32[256,2]{0,1:T(2,128)} %param.21) | copy-start | bytes 6148
  0.8 9.5 %copy-start.4 = (bf16[3,2048]{1,0:T(4,128)(2,1)S(1)}, bf16[3,2048]{1,0:T(4,128)(2,1)}, u32[]{:S(2)}) copy-start(bf16[3,2048]{1,0:T(4,128)(2,1)} %param.17) | copy-start | bytes 36868
  0.8 9.5 %copy-start.5 = (f32[3,2048]{1,0:T(4,128)S(1)}, f32[3,2048]{1,0:T(4,128)}, u32[]{:S(2)}) copy-start(f32[3,2048]{1,0:T(4,128)} %param.20) | copy-start | bytes 73732
  0.8 10.7 %copy-start.8 = (s32[256]{0:T(256)S(1)}, s32[256]{0:T(256)}, u32[]{:S(2)}) copy-start(s32[256]{0:T(256)} %param.18) | copy-start | bytes 3076
  0.8 10.6 %collective-permute-start = (f32[2]{0:T(128)S(1)}, f32[2]{0:T(128)S(1)}, u32[]{:S(2)}, u32[]{:S(2)}) collective-permute-start(f32[2]{0:T(128)S(1)} %slice.43), channel_id=1, source_target_pairs={{0,1},{1,2},{2,3},{3,4},{4,5},{5,6},{6,7},{7,8},{8,9},{9,10},{10,1... | collective-permute-start | bytes 32 | tf_op jit(solution)/shard_map/ppermute | solution.py:16
  6.6 5.0 %collective-permute-start.1 = (f32[2,2048]{1,0:T(2,128)S(1)}, f32[2,2048]{1,0:T(2,128)S(1)}, u32[]{:S(2)}, u32[]{:S(2)}) collective-permute-start(f32[2,2048]{1,0:T(2,128)S(1)} %slice.62), channel_id=1, source_target_pairs={{0,1},{1,2},{2,3},{3,4},{4,5},{5,6},{6,7},{7,8},{8,9},{9,10},{10,1... | collective-permute-start | bytes 49160 | tf_op jit(solution)/shard_map/ppermute | solution.py:16
  11.6 6.8 %copy-start = (bf16[256,2048]{1,0:T(8,128)(2,1)S(1)}, bf16[256,2048]{1,0:T(8,128)(2,1)}, u32[]{:S(2)}) copy-start(bf16[256,2048]{1,0:T(8,128)(2,1)} %param.13) | copy-start | bytes 3145732
  18.3 1.0 copy-start.2
  161.1 5.8 %copy-start.7 = (f32[256,2]{0,1:T(2,128)S(1)}, f32[256,2]{0,1:T(2,128)}, u32[]{:S(2)}) copy-start(f32[256,2]{0,1:T(2,128)} %param.22) | copy-start | bytes 6148
  161.1 75.1 %all-to-all-start.1 = ((bf16[16,48,2048]{2,1,0:T(8,128)(2,1)}), bf16[16,48,2048]{2,1,0:T(8,128)(2,1)S(1)}, u32[]{:S(2)}, u32[]{:S(2)}) async-start(bf16[16,48,2048]{2,1,0:T(8,128)(2,1)} %bitcast.54), calls=%async_computation.1 | async-start | bytes 6291456 | tf_op jit(solution)/shard_map/all_to_all | solution.py:118
  262.1 1.2 copy-start.1
  262.1 1.5 copy-start.3
where the time goes:
time: 266 us; the launch traced here: 265 us
  blocking collectives  74.9 us (28%)
  waiting for transfers between devices  69.2 us (26%)
  matrix products  66.6 us (25%)
  local copies, waits for them, and re-layouts  24.3 us (9%)
  other arithmetic  19 us (7%)
  starting transfers between devices  11 us (4%)
    all_to_all x1, blocking collectives, per_device(): lax.all_to_all(outgoing, 'sp', split_axis=0, concat_axis=0, tiled=True)  74.9 us
    all_to_all x1, waiting for transfers between devices, per_device(): lax.all_to_all(results, 'sp', split_axis=0, concat_axis=0, tiled=True)  69.2 us
    dot_general x1, matrix products, per_device(): jnp.dot(block_rows, w_down[0], preferred_element_type=jnp.float32)  40.4 us
    dot_general x1, matrix products, expert_hidden(): jnp.dot(picked_rows, w_gate[0], preferred_element_type=jnp.float32)  19.3 us
    gather x1, local copies, waits for them, and re-layouts, per_device(): picked = returned[my_routes, slot_rank]  11.5 us
    reduce_sum x1, other arithmetic, per_device(): combined = jnp.sum(shares[:, :, None] * picked.astype(jnp.float32), axis=1)  8.89 us
    dot_general x1, matrix products, per_device(): jnp.dot(block_rows, out_weight, preferred_element_type=jnp.float32)  6.79 us
    ppermute x2, starting transfers between devices, passed_along(): return lax.ppermute(block, axis, route)  5.78 us
  transfers between devices with their start and end apart: 3, of which 1 were waited for; matrix products, arithmetic and copies ran while one was open for 2% of the time, Pallas kernels for 0%

commit v1 on v0

--- a/solution.py
+++ b/solution.py
@@ -1,6 +1,11 @@
+import functools
+
 import jax
 import jax.numpy as jnp
+import numpy as np
 from jax import lax
+from jax.experimental import pallas as pl
+from jax.experimental.pallas import tpu as pltpu
 from jax.sharding import PartitionSpec as P
 
 TAPS = 3
@@ -50,7 +55,7 @@
     return (jax.nn.silu(gate_proj) * up_proj).astype(jnp.bfloat16)
 
 
-def per_device(
+def per_device_split(
     resid,
     gate_b,
     gate_c,
@@ -122,7 +127,218 @@
     return (stream + rms_scale(combined, norm_gains[2])).astype(jnp.bfloat16)
 
 
+MESH = pl.DeviceIdType.MESH
+
+
+def flipped(me, distance, n):
+    out, bit = 0, 1
+    while bit < n:
+        digit = (me // bit) % 2
+        if distance & bit:
+            digit = 1 - digit
+        out = out + digit * bit
+        bit *= 2
+    return out
+
+
+def visiting_order(n):
+    quarter = n // 4
+    order = list(range(n // 2, n)) + list(range(quarter, n // 2)) + list(range(1, quarter)) + [0]
+    groups = [(0, quarter), (quarter, quarter), (2 * quarter, n - 2 * quarter)]
+    return order, groups
+
+
+def expert_kernel(
+    n, cap, order, groups, tile,
+    rows_hbm, gate_hbm, up_hbm, down_hbm, back_hbm,
+    gate_v, up_v, down_v, arrived, hidden, weight_sem, send_sem, recv_sem, back_send, back_recv, own_sem,
+):
+    me = lax.axis_index("sp")
+    units = gate_v.shape[1]
+    width = down_v.shape[1]
+    loads = [
+        pltpu.make_async_copy(src.at[0], dst, weight_sem.at[i])
+        for i, (src, dst) in enumerate(((gate_hbm, gate_v), (up_hbm, up_v), (down_hbm, down_v)))
+    ]
+    barrier = pltpu.get_barrier_semaphore()
+    for distance in order:
+        if distance:
+            pl.semaphore_signal(
+                barrier, inc=1, device_id={"sp": flipped(me, distance, n)}, device_id_type=MESH
+            )
+    pl.semaphore_wait(barrier, n - 1)
+
+    def block(ref, i):
+        return ref.at[pl.ds(i * cap, cap)]
+
+    def remote(src, dst, i, sent, got):
+        return pltpu.make_async_remote_copy(
+            src_ref=block(src, i),
+            dst_ref=block(dst, i),
+            send_sem=sent.at[i],
+            recv_sem=got.at[i],
+            device_id={"sp": flipped(me, order[i], n)},
+            device_id_type=MESH,
+        )
+
+    own = n - 1
+    outbound = [remote(rows_hbm, arrived, i, send_sem, recv_sem) for i in range(own)]
+    for copy in outbound:
+        copy.start()
+    own_in = pltpu.make_async_copy(block(rows_hbm, own), block(arrived, own), own_sem.at[0])
+    own_in.start()
+    for copy in loads:
+        copy.start()
+    inbound = []
+    for first, count in groups:
+        for i in range(first, first + count):
+            if i == own:
+                own_in.wait()
+            else:
+                outbound[i].wait_recv()
+        if first == 0:
+            loads[0].wait()
+            loads[1].wait()
+        rows = pl.ds(first * cap, count * cap)
+        picked = pl.ds(0, count * cap)
+
+        @pl.loop(0, units // tile)
+        def _(t):
+            cols = pl.ds(pl.multiple_of(t * tile, tile), tile)
+            x = arrived[rows, :]
+            g = jnp.dot(x, gate_v[:, cols], preferred_element_type=jnp.float32)
+            u = jnp.dot(x, up_v[:, cols], preferred_element_type=jnp.float32)
+            hidden[picked, cols] = (g / (1.0 + jnp.exp(-g)) * u).astype(jnp.bfloat16)
+
+        if first == 0:
+            loads[2].wait()
+
+        @pl.loop(0, width // tile)
+        def _(t):
+            cols = pl.ds(pl.multiple_of(t * tile, tile), tile)
+            arrived[rows, cols] = jnp.dot(
+                hidden[picked, :], down_v[:, cols], preferred_element_type=jnp.float32
+            ).astype(jnp.bfloat16)
+
+        for i in range(first, first + count):
+            if i == own:
+                copy = pltpu.make_async_copy(block(arrived, own), block(back_hbm, own), own_sem.at[1])
+            else:
+                copy = remote(arrived, back_hbm, i, back_send, back_recv)
+            copy.start()
+            inbound.append(copy)
+    for copy in outbound:
+        copy.wait_send()
+    for copy in inbound:
+        copy.wait()
+
+
+def run_experts(outgoing, w_gate, w_up, w_down, n, cap, order, groups):
+    model_width, units = w_gate.shape[1], w_gate.shape[2]
+    most = max(count for _, count in groups) * cap
+    tile = 512
+    total_rows = n * cap
+    dma = pltpu.SemaphoreType.DMA
+    return pl.pallas_call(
+        functools.partial(expert_kernel, n, cap, order, groups, tile),
+        out_shape=jax.ShapeDtypeStruct(outgoing.shape, jnp.bfloat16),
+        in_specs=[pl.BlockSpec(memory_space=pl.ANY)] * 4,
+        out_specs=pl.BlockSpec(memory_space=pl.ANY),
+        scratch_shapes=[
+            pltpu.VMEM((model_width, units), jnp.bfloat16),
+            pltpu.VMEM((model_width, units), jnp.bfloat16),
+            pltpu.VMEM((units, model_width), jnp.bfloat16),
+            pltpu.VMEM((total_rows, model_width), jnp.bfloat16),
+            pltpu.VMEM((most, units), jnp.bfloat16),
+            dma((3,)),
+            dma((n,)),
+            dma((n,)),
+            dma((n,)),
+            dma((n,)),
+            dma((2,)),
+        ],
+        compiler_params=pltpu.CompilerParams(
+            collective_id=0, has_side_effects=True, vmem_limit_bytes=64 * 1024 * 1000
+        ),
+        cost_estimate=pl.CostEstimate(
+            flops=6 * total_rows * model_width * units,
+            bytes_accessed=6 * model_width * units,
+            transcendentals=total_rows * units,
+        ),
+    )(outgoing, w_gate, w_up, w_down)
+
+
+def per_device_whole(
+    resid, gate_b, gate_c, value, taps, doc_ids, out_weight, norm_gains,
+    routes, route_weights, w_gate, w_up, w_down,
+):
+    tok_dev = gate_b.shape[0]
+    rows_blk, model_width = resid.shape
+    experts = lax.axis_size("sp")
+    capacity = max(2, 3 * TOP * rows_blk // (2 * experts))
+    tap_reach = TAPS - 1
+    order, groups = visiting_order(experts)
+    product = gate_c.astype(jnp.float32) * value.astype(jnp.float32)
+    id_values = doc_ids.astype(jnp.float32)
+    id_row = jnp.pad(id_values[tok_dev - tap_reach :], (0, model_width - tap_reach))
+    handed = passed_along(
+        jnp.concatenate([product[tok_dev - tap_reach :], id_row[None]], axis=0), "sp", 1
+    )
+    ext_rows = jnp.concatenate([handed[:tap_reach], product], axis=0)
+    ext_ids = jnp.concatenate([handed[tap_reach, :tap_reach], id_values], axis=0)
+    tap_weights = taps.astype(jnp.float32)
+    convolved = tap_weights[0] * product
+    for distance in range(1, TAPS):
+        earlier = ext_rows[tap_reach - distance : tap_reach - distance + tok_dev]
+        same_doc = ext_ids[tap_reach - distance : tap_reach - distance + tok_dev] == id_values
+        convolved = convolved + jnp.where(same_doc[:, None], tap_weights[distance] * earlier, 0.0)
+    mixed_rows = (gate_b.astype(jnp.float32) * convolved).astype(jnp.bfloat16)
+    projected = (
+        jnp.dot(mixed_rows, out_weight, preferred_element_type=jnp.float32)
+        .astype(jnp.bfloat16)
+        .astype(jnp.float32)
+    )
+    stream = resid.astype(jnp.float32) + rms_scale(projected, norm_gains[0])
+    normed = rms_scale(stream, norm_gains[1]).astype(jnp.bfloat16)
+
+    def dot32(a, b):
+        return jnp.dot(a, b, preferred_element_type=jnp.float32)
+
+    visited = jnp.asarray(np.array(order, np.int32)) ^ lax.axis_index("sp")
+    names = routes[:, :, None] == visited[None, None, :]
+    hit = jnp.any(names, axis=1)
+    earlier_rows = jnp.asarray(np.tril(np.ones((rows_blk, rows_blk), np.float32), -1), jnp.bfloat16)
+    rank = dot32(earlier_rows, hit.astype(jnp.bfloat16))
+    place = jnp.where(hit, rank + 1.0, 0.0).astype(jnp.bfloat16)
+    slots = np.arange(experts * capacity)
+    spread = jnp.asarray(
+        (slots[None, :] // capacity == np.arange(experts)[:, None]).astype(np.float32), jnp.bfloat16
+    )
+    wanted = jnp.asarray((slots % capacity + 1).astype(np.float32))
+    chosen = dot32(place, spread) == wanted[None, :]
+    outgoing = lax.dot_general(
+        chosen.astype(jnp.bfloat16),
+        normed,
+        (((0,), (0,)), ((), ())),
+        preferred_element_type=jnp.float32,
+    ).astype(jnp.bfloat16)
+    shares = route_weights / jnp.sum(route_weights, axis=1, keepdims=True)
+    share_of = jnp.sum(jnp.where(names, shares[:, :, None], 0.0), axis=1)
+    share_high = lax.reduce_precision(share_of, 8, 7)
+    share_low = share_of - share_high
+    parts = [
+        jnp.where(chosen, dot32(part.astype(jnp.bfloat16), spread), 0.0).astype(jnp.bfloat16)
+        for part in (share_high, share_low)
+    ]
+    returned = run_experts(outgoing, w_gate, w_up, w_down, experts, capacity, order, groups)
+    combined = dot32(parts[0], returned) + dot32(parts[1], returned)
+    return (stream + rms_scale(combined, norm_gains[2])).astype(jnp.bfloat16)
+
+
 def solution(mesh):
+    experts = mesh.shape["sp"]
+    whole_tokens = mesh.shape["tp"] == 1 and experts >= 8 and experts & (experts - 1) == 0
+    per_device = per_device_whole if whole_tokens else per_device_split
     return jax.shard_map(
         per_device,
         mesh=mesh,

time: 266 us -> 193 us (0.73)
  the two profiles are of different devices: /device:TPU:11 before, /device:TPU:7 now
where the time goes in v1:
time: 193 us; the launch traced here: 192 us
  Pallas kernels  162 us (84%)
  matrix products  19 us (10%)
  other arithmetic  6.84 us (4%)
  starting transfers between devices  3.74 us (2%)
    pallas_call x1, Pallas kernels, run_experts(): pl.pallas_call(functools.partial(expert_kernel, n, cap, order, groups, ti...  162 us
    dot_general x3, matrix products, dot32(): return jnp.dot(a, b, preferred_element_type=jnp.float32)  9.16 us
    dot_general x1, matrix products, per_device_whole(): jnp.dot(mixed_rows, out_weight, preferred_element_type=jnp.float32)  6.79 us
  transfers between devices with their start and end apart: 1, of which 1 were waited for; matrix products, arithmetic and copies ran while one was open for 0% of the time, Pallas kernels for 0%

profile of v1, /device:TPU:7, one launch (start us, length us, event | category | flops | bytes accessed | tf_op | source)
XLA Modules:
  0.0 191.9 jit_solution(13086639063499579033)
XLA Ops:
  0.0 0.0 copy-start.11
  0.1 2.0 %convert_multiply_fusion.2 = f32[256,2048]{1,0:T(8,128)S(1)} fusion(bf16[256,2048]{1,0:T(8,128)(2,1)} %param.20, bf16[256,2048]{1,0:T(8,128)(2,1)} %param.19), kind=kLoop, calls=%fused_computation.24 | loop fusion | flops 1572864 | bytes 4194304 | tf_op jit(solution)/shard_map/mul | solution.py:281
  2.1 0.1 slice.44
  2.2 3.7 %collective-permute-start = (f32[3,2048]{1,0:T(4,128)S(1)}, f32[3,2048]{1,0:T(4,128)S(1)}, u32[]{:S(2)}, u32[]{:S(2)}) collective-permute-start(f32[3,2048]{1,0:T(4,128)S(1)} %pad_maximum_fusion.1), channel_id=1, source_target_pairs={{0,1},{1,2},{2,3},{3,4},{4,5},{5,6},{6,7},{7,8},{8,9},{9,10},{10,1... | collective-permute-start | bytes 73736 | tf_op jit(solution)/shard_map/ppermute | solution.py:21
  6.1 0.0 copy-done.6
  6.1 0.0 copy-done.7
  6.1 0.1 compare_reduce_fusion
  6.2 0.0 copy-done.9
  6.2 0.0 copy-done.11
  6.2 0.5 convolution_compare_fusion
  6.8 0.1 fusion.31
  6.8 0.2 collective-permute-done
  7.0 0.1 pad_maximum_fusion.2
  7.1 0.1 slice_compare_fusion.1
  7.2 0.0 copy-start.1
  7.2 6.8 %fusion.7 = (f32[256]{0:T(256)S(1)}, bf16[256,2048]{1,0:T(8,128)(2,1)S(1)}) fusion(bf16[2048,2048]{1,0:T(8,128)(2,1)} %param.23, f32[2,2048]{1,0:T(2,128)S(1)} %slice.60, f32[256,2048]{1,0:T(8,128)S(1)} %convert_multiply_fusion.2, bf16[256,2048]{1,0:T(8,128)(2,1)} %param.18, f32[2048]{0:T(1024)S(1)} %bitcast.34, f32[2048]{0:T(1024)S(1)} %bitcast.33, ...), kind=kOutput, calls=%fused_computation.14 | convolution fusion | flops 2155872000 | bytes 12625408 | tf_op jit(solution)/shard_map/dot_general | solution.py:297
  14.0 0.0 copy-start.2
  14.0 0.6 multiply_reduce_fusion.1
  14.6 0.3 copy-done.2
  14.9 3.0 %convolution_convert_fusion.rows_hbm = bf16[768,2048]{1,0:T(8,128)(2,1)} fusion(pred[256,768]{1,0:T(32,128)(4,1)S(1)} %convolution_compare_fusion, bf16[256,2048]{1,0:T(8,128)(2,1)S(1)} %get-tuple-element.14, bf16[256,2048]{1,0:T(8,128)(2,1)S(1)} %copy-done.1, f32[2048]{0:T(1024)S(1)} %bitcast.31, f32[256]{0:T(256)S(1)} %add_rsqrt_fusion.1, ...), kind=kOutput, calls=%fused_computation | convolution fusion | flops 811073536 | bytes 5457920 | tf_op jit(solution)/shard_map/dot_general | solution.py:319
  18.0 161.5 %shard_map.163 = bf16[768,2048]{1,0:T(8,128)(2,1)} custom-call(bf16[768,2048]{1,0:T(8,128)(2,1)} %convolution_convert_fusion.rows_hbm, bf16[1,2048,4096]{2,1,0:T(8,128)(2,1)} %gate_hbm.1, bf16[1,2048,4096]{2,1,0:T(8,128)(2,1)} %up_hbm.1, bf16[1,4096,2048]{2,1,0:T(8,128)(2,1)} %down_hbm.1), custom_call_target="tpu_custom_call" | custom-call | flops 38654705664 | bytes 50331648 | tf_op jit(solution)/shard_map/pallas_call | solution.py:242
  179.5 4.5 %fusion.14 = f32[256,2048]{1,0:T(8,128)} fusion(bf16[768,2048]{1,0:T(8,128)(2,1)} %shard_map.163, pred[256,768]{1,0:T(32,128)(4,1)S(1)} %convolution_compare_fusion, bf16[16,768]{1,0:T(8,128)(2,1)S(1)} %copy-done.3, f32[256,16]{0,1:T(8,128)S(1)} %fusion.31), kind=kOutput, calls=%fused_computation.30 | convolution fusion | flops 811999232 | bytes 5480448 | tf_op jit(solution)/shard_map/dot_general | solution.py:305
  184.0 4.1 %multiply_reduce_fusion = (f32[256]{0:T(256)S(1)}, f32[256,2048]{1,0:T(8,128)}) fusion(f32[256,2048]{1,0:T(8,128)} %fusion.14, bf16[768,2048]{1,0:T(8,128)(2,1)S(1)} %copy-done, pred[256,768]{1,0:T(32,128)(4,1)S(1)} %convolution_compare_fusion, bf16[16,768]{1,0:T(8,128)(2,1)S(1)} %copy-done.3, f32[256,16]{0,1:T(8,128)S(1)} %fusion.31), kind=kOutput, calls=%fused_computation.21 | convolution fusion | flops 813575936 | bytes 7578624 | tf_op jit(solution)/shard_map/dot_general | solution.py:305
  188.1 3.8 %add_convert_fusion = bf16[256,2048]{1,0:T(8,128)(2,1)} fusion(f32[256,2048]{1,0:T(8,128)} %get-tuple-element.16, bf16[256,2048]{1,0:T(8,128)(2,1)} %copy-done.2, bf16[256,2048]{1,0:T(8,128)(2,1)} %param.17, f32[2048]{0:T(1024)S(1)} %bitcast.29, f32[256]{0:T(256)S(1)} %add_rsqrt_fusion, f32[2048]{0:T(1024)S(1)} %bitcast.28, f32[256]{0:T(256)S(1)} %add_rsqrt_fusion.2), kind=kLoop, calls=%fused_computation.20 | loop fusion | flops 4718592 | bytes 5261312 | tf_op jit(solution)/shard_map/convert_element_type | solution.py:335
  (30 shorter events, 0.2 us)
Async XLA Ops:
  0.0 6.1 %copy-start.10 = (s32[16]{0:T(128)S(1)}, s32[16]{0:T(128)}, u32[]{:S(2)}) copy-start(s32[16]{0:T(128)} %constant.27.clone) | copy-start | bytes 196
  0.0 6.2 %copy-start.3 = (bf16[16,768]{1,0:T(8,128)(2,1)S(1)}, bf16[16,768]{1,0:T(8,128)(2,1)}, u32[]{:S(2)}) copy-start(bf16[16,768]{1,0:T(8,128)(2,1)} %constant.29.clone) | copy-start | bytes 73732
  0.0 6.2 %copy-start.9 = (bf16[256,256]{1,0:T(8,128)(2,1)S(1)}, bf16[256,256]{1,0:T(8,128)(2,1)}, u32[]{:S(2)}) copy-start(bf16[256,256]{1,0:T(8,128)(2,1)} %constant.28.clone) | copy-start | bytes 393220
  0.0 6.2 %copy-start.11 = (f32[768]{0:T(1024)S(1)}, f32[768]{0:T(1024)}, u32[]{:S(2)}) copy-start(f32[768]{0:T(1024)} %constant.30.clone) | copy-start | bytes 9220
  0.0 2.1 %copy-start.8 = (s32[256]{0:T(256)S(1)}, s32[256]{0:T(256)}, u32[]{:S(2)}) copy-start(s32[256]{0:T(256)} %param.22) | copy-start | bytes 3076
  0.0 6.0 %copy-start.4 = (bf16[3,2048]{1,0:T(4,128)(2,1)S(1)}, bf16[3,2048]{1,0:T(4,128)(2,1)}, u32[]{:S(2)}) copy-start(bf16[3,2048]{1,0:T(4,128)(2,1)} %param.21) | copy-start | bytes 36868
  0.0 6.0 %copy-start.5 = (f32[3,2048]{1,0:T(4,128)S(1)}, f32[3,2048]{1,0:T(4,128)}, u32[]{:S(2)}) copy-start(f32[3,2048]{1,0:T(4,128)} %param.24) | copy-start | bytes 73732
  0.1 6.0 %copy-start.6 = (f32[256,2]{0,1:T(2,128)S(1)}, f32[256,2]{0,1:T(2,128)}, u32[]{:S(2)}) copy-start(f32[256,2]{0,1:T(2,128)} %param.26) | copy-start | bytes 6148
  0.1 6.1 %copy-start.7 = (s32[256,2]{0,1:T(2,128)S(1)}, s32[256,2]{0,1:T(2,128)}, u32[]{:S(2)}) copy-start(s32[256,2]{0,1:T(2,128)} %param.25) | copy-start | bytes 6148
  2.2 4.7 %collective-permute-start = (f32[3,2048]{1,0:T(4,128)S(1)}, f32[3,2048]{1,0:T(4,128)S(1)}, u32[]{:S(2)}, u32[]{:S(2)}) collective-permute-start(f32[3,2048]{1,0:T(4,128)S(1)} %pad_maximum_fusion.1), channel_id=1, source_target_pairs={{0,1},{1,2},{2,3},{3,4},{4,5},{5,6},{6,7},{7,8},{8,9},{9,10},{10,1... | collective-permute-start | bytes 73736 | tf_op jit(solution)/shard_map/ppermute | solution.py:21
  7.2 6.8 %copy-start.1 = (bf16[256,2048]{1,0:T(8,128)(2,1)S(1)}, bf16[256,2048]{1,0:T(8,128)(2,1)}, u32[]{:S(2)}) copy-start(bf16[256,2048]{1,0:T(8,128)(2,1)} %param.17) | copy-start | bytes 3145732
  14.0 1.0 copy-start.2
  179.5 4.5 %copy-start = (bf16[768,2048]{1,0:T(8,128)(2,1)S(1)}, bf16[768,2048]{1,0:T(8,128)(2,1)}, u32[]{:S(2)}) copy-start(bf16[768,2048]{1,0:T(8,128)(2,1)} %shard_map.163) | copy-start | bytes 9437188

commit v2 on v1

--- a/solution.py
+++ b/solution.py
@@ -143,29 +143,41 @@
 
 def visiting_order(n):
     quarter = n // 4
-    order = list(range(n // 2, n)) + list(range(quarter, n // 2)) + list(range(1, quarter)) + [0]
-    groups = [(0, quarter), (quarter, quarter), (2 * quarter, n - 2 * quarter)]
-    return order, groups
+    order = (
+        list(range(quarter)) + list(range(n // 2, n)) + list(range(quarter, n // 2))
+    )
+    return order, quarter
 
 
 def expert_kernel(
-    n, cap, order, groups, tile,
-    rows_hbm, gate_hbm, up_hbm, down_hbm, back_hbm,
-    gate_v, up_v, down_v, arrived, hidden, weight_sem, send_sem, recv_sem, back_send, back_recv, own_sem,
+    n, cap, order, group, tile, down_tile,
+    rows_hbm, gate_hbm, up_hbm, down_hbm, weights_v, stream_hbm, gain_v, out_v,
+    gate_v, up_v, down_v, arrived, hidden, back, stream_v, total,
+    gate_sem, up_sem, down_sem, send_sem, recv_sem, back_send, back_recv, own_sem,
 ):
     me = lax.axis_index("sp")
     units = gate_v.shape[1]
     width = down_v.shape[1]
-    loads = [
-        pltpu.make_async_copy(src.at[0], dst, weight_sem.at[i])
-        for i, (src, dst) in enumerate(((gate_hbm, gate_v), (up_hbm, up_v), (down_hbm, down_v)))
-    ]
+
+    def columns(t, size):
+        return pl.ds(pl.multiple_of(t * size, size), size)
+
+    def load(src, dst, sem, t, size):
+        cols = columns(t, size)
+        return pltpu.make_async_copy(src.at[0, :, cols], dst.at[:, cols], sem.at[t])
+
     barrier = pltpu.get_barrier_semaphore()
-    for distance in order:
-        if distance:
-            pl.semaphore_signal(
-                barrier, inc=1, device_id={"sp": flipped(me, distance, n)}, device_id_type=MESH
-            )
+    for distance in order[1:]:
+        pl.semaphore_signal(
+            barrier, inc=1, device_id={"sp": flipped(me, distance, n)}, device_id_type=MESH
+        )
+    stream_in = pltpu.make_async_copy(stream_hbm, stream_v, own_sem.at[2])
+    for t in range(units // tile):
+        load(gate_hbm, gate_v, gate_sem, t, tile).start()
+        load(up_hbm, up_v, up_sem, t, tile).start()
+    for t in range(width // down_tile):
+        load(down_hbm, down_v, down_sem, t, down_tile).start()
+    stream_in.start()
     pl.semaphore_wait(barrier, n - 1)
 
     def block(ref, i):
@@ -181,91 +193,108 @@
             device_id_type=MESH,
         )
 
-    own = n - 1
-    outbound = [remote(rows_hbm, arrived, i, send_sem, recv_sem) for i in range(own)]
+    outbound = [pltpu.make_async_copy(block(rows_hbm, 0), block(arrived, 0), own_sem.at[0])]
+    outbound += [remote(rows_hbm, arrived, i, send_sem, recv_sem) for i in range(1, n)]
     for copy in outbound:
         copy.start()
-    own_in = pltpu.make_async_copy(block(rows_hbm, own), block(arrived, own), own_sem.at[0])
-    own_in.start()
-    for copy in loads:
-        copy.start()
     inbound = []
-    for first, count in groups:
-        for i in range(first, first + count):
-            if i == own:
-                own_in.wait()
+    for first in range(0, n, group):
+        for i in range(first, first + group):
+            if i == 0:
+                outbound[0].wait()
             else:
                 outbound[i].wait_recv()
-        if first == 0:
-            loads[0].wait()
-            loads[1].wait()
-        rows = pl.ds(first * cap, count * cap)
-        picked = pl.ds(0, count * cap)
+        rows = pl.ds(first * cap, group * cap)
 
         @pl.loop(0, units // tile)
         def _(t):
-            cols = pl.ds(pl.multiple_of(t * tile, tile), tile)
+            if first == 0:
+                load(gate_hbm, gate_v, gate_sem, t, tile).wait()
+                load(up_hbm, up_v, up_sem, t, tile).wait()
+            cols = columns(t, tile)
             x = arrived[rows, :]
             g = jnp.dot(x, gate_v[:, cols], preferred_element_type=jnp.float32)
             u = jnp.dot(x, up_v[:, cols], preferred_element_type=jnp.float32)
-            hidden[picked, cols] = (g / (1.0 + jnp.exp(-g)) * u).astype(jnp.bfloat16)
-
-        if first == 0:
-            loads[2].wait()
-
-        @pl.loop(0, width // tile)
+            hidden[:, cols] = (g / (1.0 + jnp.exp(-g)) * u).astype(jnp.bfloat16)
+
+        @pl.loop(0, width // down_tile)
         def _(t):
-            cols = pl.ds(pl.multiple_of(t * tile, tile), tile)
+            if first == 0:
+                load(down_hbm, down_v, down_sem, t, down_tile).wait()
+            cols = columns(t, down_tile)
             arrived[rows, cols] = jnp.dot(
-                hidden[picked, :], down_v[:, cols], preferred_element_type=jnp.float32
+                hidden[...], down_v[:, cols], preferred_element_type=jnp.float32
             ).astype(jnp.bfloat16)
 
-        for i in range(first, first + count):
-            if i == own:
-                copy = pltpu.make_async_copy(block(arrived, own), block(back_hbm, own), own_sem.at[1])
+        for i in range(first, first + group):
+            if i == 0:
+                copy = pltpu.make_async_copy(block(arrived, 0), block(back, 0), own_sem.at[1])
             else:
-                copy = remote(arrived, back_hbm, i, back_send, back_recv)
+                copy = remote(arrived, back, i, back_send, back_recv)
             copy.start()
             inbound.append(copy)
-    for copy in outbound:
+    stream_in.wait()
+    inbound[0].wait()
+    for copy in inbound[1:]:
+        copy.wait_recv()
+
+    @pl.loop(0, width // down_tile)
+    def _(t):
+        cols = columns(t, down_tile)
+        total[:, cols] = jnp.dot(weights_v[...], back[:, cols], preferred_element_type=jnp.float32)
+
+    part = 32
+
+    @pl.loop(0, total.shape[0] // part)
+    def _(t):
+        some = pl.ds(pl.multiple_of(t * part, part), part)
+        out_v[some, :] = (stream_v[some, :] + rms_scale(total[some, :], gain_v[...])).astype(
+            out_v.dtype
+        )
+
+    for copy in outbound[1:] + inbound[1:]:
         copy.wait_send()
-    for copy in inbound:
-        copy.wait()
-
-
-def run_experts(outgoing, w_gate, w_up, w_down, n, cap, order, groups):
+
+
+def run_experts(outgoing, w_gate, w_up, w_down, weights, stream, gain, n, cap, order, group):
     model_width, units = w_gate.shape[1], w_gate.shape[2]
-    most = max(count for _, count in groups) * cap
-    tile = 512
+    tile, down_tile = 512, 512
     total_rows = n * cap
     dma = pltpu.SemaphoreType.DMA
+    anywhere = pl.BlockSpec(memory_space=pl.ANY)
+    near = pl.BlockSpec(memory_space=pltpu.VMEM)
     return pl.pallas_call(
-        functools.partial(expert_kernel, n, cap, order, groups, tile),
-        out_shape=jax.ShapeDtypeStruct(outgoing.shape, jnp.bfloat16),
-        in_specs=[pl.BlockSpec(memory_space=pl.ANY)] * 4,
-        out_specs=pl.BlockSpec(memory_space=pl.ANY),
+        functools.partial(expert_kernel, n, cap, order, group, tile, down_tile),
+        out_shape=jax.ShapeDtypeStruct(stream.shape, jnp.bfloat16),
+        in_specs=[anywhere] * 4 + [near, anywhere, near],
+        out_specs=near,
         scratch_shapes=[
             pltpu.VMEM((model_width, units), jnp.bfloat16),
             pltpu.VMEM((model_width, units), jnp.bfloat16),
             pltpu.VMEM((units, model_width), jnp.bfloat16),
             pltpu.VMEM((total_rows, model_width), jnp.bfloat16),
-            pltpu.VMEM((most, units), jnp.bfloat16),
-            dma((3,)),
+            pltpu.VMEM((group * cap, units), jnp.bfloat16),
+            pltpu.VMEM((total_rows, model_width), jnp.bfloat16),
+            pltpu.VMEM(stream.shape, jnp.float32),
+            pltpu.VMEM(stream.shape, jnp.float32),
+            dma((units // tile,)),
+            dma((units // tile,)),
+            dma((model_width // down_tile,)),
             dma((n,)),
             dma((n,)),
             dma((n,)),
             dma((n,)),
-            dma((2,)),
+            dma((3,)),
         ],
         compiler_params=pltpu.CompilerParams(
-            collective_id=0, has_side_effects=True, vmem_limit_bytes=64 * 1024 * 1000
+            collective_id=0, has_side_effects=True, vmem_limit_bytes=67043328
         ),
         cost_estimate=pl.CostEstimate(
             flops=6 * total_rows * model_width * units,
             bytes_accessed=6 * model_width * units,
             transcendentals=total_rows * units,
         ),
-    )(outgoing, w_gate, w_up, w_down)
+    )(outgoing, w_gate, w_up, w_down, weights, stream, gain)
 
 
 def per_device_whole(
@@ -277,7 +306,7 @@
     experts = lax.axis_size("sp")
     capacity = max(2, 3 * TOP * rows_blk // (2 * experts))
     tap_reach = TAPS - 1
-    order, groups = visiting_order(experts)
+    order, group = visiting_order(experts)
     product = gate_c.astype(jnp.float32) * value.astype(jnp.float32)
     id_values = doc_ids.astype(jnp.float32)
     id_row = jnp.pad(id_values[tok_dev - tap_reach :], (0, model_width - tap_reach))
@@ -324,15 +353,10 @@
     ).astype(jnp.bfloat16)
     shares = route_weights / jnp.sum(route_weights, axis=1, keepdims=True)
     share_of = jnp.sum(jnp.where(names, shares[:, :, None], 0.0), axis=1)
-    share_high = lax.reduce_precision(share_of, 8, 7)
-    share_low = share_of - share_high
-    parts = [
-        jnp.where(chosen, dot32(part.astype(jnp.bfloat16), spread), 0.0).astype(jnp.bfloat16)
-        for part in (share_high, share_low)
-    ]
-    returned = run_experts(outgoing, w_gate, w_up, w_down, experts, capacity, order, groups)
-    combined = dot32(parts[0], returned) + dot32(parts[1], returned)
-    return (stream + rms_scale(combined, norm_gains[2])).astype(jnp.bfloat16)
+    weights = jnp.where(chosen, dot32(share_of.astype(jnp.bfloat16), spread), 0.0).astype(jnp.bfloat16)
+    return run_experts(
+        outgoing, w_gate, w_up, w_down, weights, stream, norm_gains[2:3], experts, capacity, order, group
+    )
 
 
 def solution(mesh):

time: 193 us -> 177 us (0.917)
  matrix products: 19 us -> 11.7 us
  Pallas kernels: 162 us -> 155 us
  other arithmetic: 6.84 us -> 3.63 us
  local copies, waits for them, and re-layouts: 0.5 us -> 3.09 us
    pallas_call x1, Pallas kernels: 162 us -> 155 us  [run_experts(): pl.pallas_call(functools.partial(expert_kernel, n, cap, order, group, til...]
    dot_general x3 -> x2, matrix products: 9.16 us -> 2.44 us  [dot32(): return jnp.dot(a, b, preferred_element_type=jnp.float32)]
    convert_element_type x1 -> x0, other arithmetic: 3.81 us -> none  [per_device_whole(): return (stream + rms_scale(combined, norm_gains[2])).astype(jnp.bfloat16)]
    unnamed x24 -> x23, local copies, waits for them, and re-layouts: 0.36 us -> 2.36 us
  transfers between devices with their start and end apart: 1 -> 1, of which waited for: 1 -> 0; matrix products, arithmetic and copies ran while one was open for 0% -> 2% of each run, Pallas kernels for 0% -> 0%
where the time goes in v2:
time: 177 us
  Pallas kernels  155 us (88%)
  matrix products  11.7 us (7%)
  starting transfers between devices  3.87 us (2%)
  other arithmetic  3.63 us (2%)
  local copies, waits for them, and re-layouts  3.09 us (2%)
    pallas_call x1, Pallas kernels, run_experts(): pl.pallas_call(functools.partial(expert_kernel, n, cap, order, group, til...  155 us
    dot_general x1, matrix products, per_device_whole(): jnp.dot(mixed_rows, out_weight, preferred_element_type=jnp.float32)  6.48 us
    ppermute x1, starting transfers between devices, passed_along(): return lax.ppermute(block, axis, route)  3.87 us
  transfers between devices with their start and end apart: 1, of which 0 were waited for; matrix products, arithmetic and copies ran while one was open for 2% of the time, Pallas kernels for 0%

profile of v2, /device:TPU:7, one launch (start us, length us, event | category | flops | bytes accessed | tf_op | source)
XLA Modules:
  0.0 177.1 jit_solution(6760042493443369965)
XLA Ops:
  0.0 0.7 convert_element_type.52
  0.7 0.1 slice.44
  0.8 0.0 copy-start.3
  0.8 0.0 copy-start.10
  0.8 2.0 %convert_multiply_fusion.2 = f32[256,2048]{1,0:T(8,128)S(1)} fusion(bf16[256,2048]{1,0:T(8,128)(2,1)} %param.20, bf16[256,2048]{1,0:T(8,128)(2,1)} %param.19), kind=kLoop, calls=%fused_computation.21 | loop fusion | flops 1572864 | bytes 4194304 | tf_op jit(solution)/shard_map/mul | solution.py:310
  2.8 0.0 copy-start.7
  2.8 0.0 copy-start.8
  2.9 3.9 %collective-permute-start = (f32[3,2048]{1,0:T(4,128)S(1)}, f32[3,2048]{1,0:T(4,128)S(1)}, u32[]{:S(2)}, u32[]{:S(2)}) collective-permute-start(f32[3,2048]{1,0:T(4,128)S(1)} %pad_maximum_fusion.1), channel_id=1, source_target_pairs={{0,1},{1,2},{2,3},{3,4},{4,5},{5,6},{6,7},{7,8},{8,9},{9,10},{10,1... | collective-permute-start | bytes 73736 | tf_op jit(solution)/shard_map/ppermute | solution.py:21
  6.7 0.0 copy-done.6
  6.8 0.0 copy-done.9
  6.8 0.1 compare_reduce_fusion
  6.9 0.1 fusion.25
  7.0 0.6 fusion.34
  7.6 1.4 convolution_compare_fusion
  9.0 1.0 fusion.12.weights_v
  10.1 0.0 collective-permute-done
  10.1 0.1 pad_maximum_fusion.2
  10.2 0.1 slice_compare_fusion.1
  10.2 0.0 copy-start.1
  10.3 6.5 %fusion.7 = (f32[256]{0:T(256)S(1)}, bf16[256,2048]{1,0:T(8,128)(2,1)S(1)}) fusion(bf16[2048,2048]{1,0:T(8,128)(2,1)} %param.23, f32[2,2048]{1,0:T(2,128)S(1)} %slice.60, f32[256,2048]{1,0:T(8,128)S(1)} %convert_multiply_fusion.2, bf16[256,2048]{1,0:T(8,128)(2,1)S(1)} %copy-done.8, f32[2048]{0:T(1024)S(1)} %bitcast.28, f32[2048]{0:T(1024)S(1)} %bitcast.27, ...), kind=kOutput, calls=%fused_computation.13 | convolution fusion | flops 2155872000 | bytes 12625408 | tf_op jit(solution)/shard_map/dot_general | solution.py:326
  16.8 0.6 multiply_reduce_fusion
  17.4 2.8 %convolution_convert_fusion.rows_hbm = bf16[768,2048]{1,0:T(8,128)(2,1)} fusion(pred[256,768]{1,0:T(32,128)(4,1)S(1)} %convolution_compare_fusion, f32[256,2048]{1,0:T(8,128)S(1)} %get-tuple-element.6.stream_hbm, f32[2048]{0:T(1024)S(1)} %bitcast.23, f32[256]{0:T(256)S(1)} %add_rsqrt_fusion), kind=kOutput, calls=%fused_computation | convolution fusion | flops 808452096 | bytes 5448704 | tf_op jit(solution)/shard_map/dot_general | solution.py:348
  20.2 154.7 %shard_map.163 = bf16[256,2048]{1,0:T(8,128)(2,1)} custom-call(bf16[768,2048]{1,0:T(8,128)(2,1)} %convolution_convert_fusion.rows_hbm, bf16[1,2048,4096]{2,1,0:T(8,128)(2,1)} %gate_hbm.1, bf16[1,2048,4096]{2,1,0:T(8,128)(2,1)} %up_hbm.1, bf16[1,4096,2048]{2,1,0:T(8,128)(2,1)} %down_hbm.1, bf16[256,768]{1,0:T(8,128)(2,1)} %fusion.12.weights_v, ...), custom_call_target="tpu_custom_call" | custom-call | flops 38654705664 | bytes 50331648 | tf_op jit(solution)/shard_map/pallas_call | solution.py:266
  174.8 2.3 %copy.24 = bf16[256,2048]{1,0:T(8,128)(2,1)} copy(bf16[256,2048]{1,0:T(8,128)(2,1)} %shard_map.163) | data formatting | bytes 2097152
  (26 shorter events, 0.1 us)
Async XLA Ops:
  0.8 6.0 %copy-start.6 = (f32[256,2]{0,1:T(2,128)S(1)}, f32[256,2]{0,1:T(2,128)}, u32[]{:S(2)}) copy-start(f32[256,2]{0,1:T(2,128)} %param.26) | copy-start | bytes 6148
  0.8 6.0 %copy-start.9 = (s32[16]{0:T(128)S(1)}, s32[16]{0:T(128)}, u32[]{:S(2)}) copy-start(s32[16]{0:T(128)} %constant.26.clone) | copy-start | bytes 196
  0.8 6.0 %copy-start.5 = (s32[256,2]{0,1:T(2,128)S(1)}, s32[256,2]{0,1:T(2,128)}, u32[]{:S(2)}) copy-start(s32[256,2]{0,1:T(2,128)} %param.25) | copy-start | bytes 6148
  0.8 6.2 %copy-start.2 = (bf16[3,2048]{1,0:T(4,128)(2,1)S(1)}, bf16[3,2048]{1,0:T(4,128)(2,1)}, u32[]{:S(2)}) copy-start(bf16[3,2048]{1,0:T(4,128)(2,1)} %param.21) | copy-start | bytes 36868
  0.8 6.2 %copy-start.4 = (f32[3,2048]{1,0:T(4,128)S(1)}, f32[3,2048]{1,0:T(4,128)}, u32[]{:S(2)}) copy-start(f32[3,2048]{1,0:T(4,128)} %param.24) | copy-start | bytes 73732
  0.8 6.8 %copy-start.3 = (bf16[16,768]{1,0:T(8,128)(2,1)S(1)}, bf16[16,768]{1,0:T(8,128)(2,1)}, u32[]{:S(2)}) copy-start(bf16[16,768]{1,0:T(8,128)(2,1)} %constant.28.clone) | copy-start | bytes 73732
  0.8 6.8 %copy-start.10 = (f32[768]{0:T(1024)S(1)}, f32[768]{0:T(1024)}, u32[]{:S(2)}) copy-start(f32[768]{0:T(1024)} %constant.29.clone) | copy-start | bytes 9220
  2.8 7.4 %copy-start.7 = (s32[256]{0:T(256)S(1)}, s32[256]{0:T(256)}, u32[]{:S(2)}) copy-start(s32[256]{0:T(256)} %param.22) | copy-start | bytes 3076
  2.8 7.5 %copy-start.8 = (bf16[256,2048]{1,0:T(8,128)(2,1)S(1)}, bf16[256,2048]{1,0:T(8,128)(2,1)}, u32[]{:S(2)}) copy-start(bf16[256,2048]{1,0:T(8,128)(2,1)} %param.18) | copy-start | bytes 3145732
  2.9 7.2 %collective-permute-start = (f32[3,2048]{1,0:T(4,128)S(1)}, f32[3,2048]{1,0:T(4,128)S(1)}, u32[]{:S(2)}, u32[]{:S(2)}) collective-permute-start(f32[3,2048]{1,0:T(4,128)S(1)} %pad_maximum_fusion.1), channel_id=1, source_target_pairs={{0,1},{1,2},{2,3},{3,4},{4,5},{5,6},{6,7},{7,8},{8,9},{9,10},{10,1... | collective-permute-start | bytes 73736 | tf_op jit(solution)/shard_map/ppermute | solution.py:21
  10.2 6.5 %copy-start.1 = (bf16[256,2048]{1,0:T(8,128)(2,1)S(1)}, bf16[256,2048]{1,0:T(8,128)(2,1)}, u32[]{:S(2)}) copy-start(bf16[256,2048]{1,0:T(8,128)(2,1)} %param.17) | copy-start | bytes 3145732
  17.4 2.8 %copy-start = (f32[256,2048]{1,0:T(8,128)}, f32[256,2048]{1,0:T(8,128)S(1)}, u32[]{:S(2)}) copy-start(f32[256,2048]{1,0:T(8,128)S(1)} %get-tuple-element.6.stream_hbm) | copy-start | bytes 6291460
